TPU v7x, 256 devices: a whole 4x4x8 slice. The times are simulated.
256 devices in a mesh: ep: 32 (over z, x), tp: 8 (over y, core).
Axes of the slice: x: 4, y: 4, z: 8, core: 2. Of those that a mesh axis runs over, the one named last changes fastest.
Arguments:
- queries: bfloat16 [16384, 1024], P('ep', 'tp'), may hold values from -8 to 8
- keys_values: bfloat16 [16384, 1024], P('ep', 'tp'), may hold values from -60 to 60
- forget_cache: float32 [16, 16384], P('tp'), may hold values from -2460 to 0, as said below
- heads_gain: float32 [1024], replicated, may hold values from 0.1 to 1.9
- output_weight: bfloat16 [1024, 2048], replicated, may hold values from -0.1875 to 0.1875
- expert_tokens: bfloat16 [4096, 2048], P('ep'), may hold values from -600 to 600
- expert_gain: float32 [2048], replicated, may hold values from 0.1 to 1.9
- routes: int32 [4096, 4], P('ep'), may hold values from 0 to 31, all different within a row; in each aligned block of 128 rows (0 to 127, 128 to 255, ...) at most 32 rows name the same one
- route_logits: float32 [4096, 4], P('ep'), may hold values from -6 to 301
- gate_weight: bfloat16 [32, 2048, 2048], P('ep', None, 'tp'), may hold values from -0.5 to 0.5
- up_weight: bfloat16 [32, 2048, 2048], P('ep', None, 'tp'), may hold values from -0.5 to 0.5
- down_weight: bfloat16 [32, 2048, 2048], P('ep', 'tp'), may hold values from -0.015625 to 0.015625
Outputs:
- mixer_out: bfloat16 [16384, 2048], P(('ep', 'tp'))
- moe_out: bfloat16 [4096, 2048], P('ep', 'tp')
Inputs may be any that keep to these rules, and one draw needn't show every extreme that they name: `forget_cache`: each row never rises from one position to the next. `routes`: the 4 experts of a row differ. In each aligned block of 128 rows (one device's tokens) no expert is named more than 32 times, so slot is below 32; some expert is named exactly 32 times in some block.
All inputs are finite; a program needn't handle non-finite values.
Results may differ from a plain program's by a relative error of at most 0.017.
Values may be sent and summed in bfloat16 or wider, within the bound.
A program may use at most 128 MiB of HBM per device.

v0:
```python
import math
import jax
import jax.numpy as jnp
from jax import lax
from jax.sharding import Mesh
from jax.sharding import PartitionSpec as P

HEAD = 64
EP = ("ep_0", "ep_1")
EP_TP = ("ep_0", "ep_1", "tp")
epsilon = 1e-06
clamp_limit = 7.0
sigmoid_slope = 1.702


def gathered_by_axis(array, axes, dim):
    whole = array
    for number in range(len(axes) - 1, -1, -1):
        whole = lax.all_gather(whole, axes[number], axis=dim, tiled=True)
    return whole


def in_blocks(array, dim, devices):
    before, after = (array.shape[:dim], array.shape[dim + 1 :])
    return jnp.moveaxis(array.reshape(*before, devices, -1, *after), dim, 0)


def sent_and_summed(array, axis, dim):
    devices = lax.axis_size(axis)
    parts = lax.all_to_all(in_blocks(array, dim, devices), axis, 0, 0, tiled=True)
    return jnp.sum(parts.astype(jnp.float32), axis=0)


def scaled_rows(values, gain_vector):
    as_float = values.astype(jnp.float32)
    inverse = lax.rsqrt(jnp.mean(as_float * as_float, axis=-1, keepdims=True) + epsilon)
    return (as_float * inverse * gain_vector).astype(jnp.bfloat16)


def assign_slots(routes, experts, capacity):
    row_count, pick_count = routes.shape
    flat_routes = routes.reshape(-1)
    onehot = (flat_routes[:, None] == jnp.arange(experts, dtype=jnp.int32)[None, :]).astype(
        jnp.int32
    )
    earlier = jnp.cumsum(onehot, axis=0) - onehot
    slot_rank = jnp.sum(earlier * onehot, axis=1)
    position = flat_routes * capacity + slot_rank
    owner_row = jnp.arange(row_count * pick_count, dtype=jnp.int32) // pick_count
    slot_token = jnp.full((experts * capacity,), row_count, jnp.int32).at[position].set(owner_row)
    return (position.reshape(row_count, pick_count), slot_token)


def body(
    queries,
    keys_values,
    forget_cache,
    heads_gain,
    output_weight,
    expert_tokens,
    expert_gain,
    routes,
    route_logits,
    gate_weight,
    up_weight,
    down_weight,
):
    row_count = queries.shape[0]
    query_count = queries.shape[1] // HEAD
    key_count = keys_values.shape[1] // (2 * HEAD)
    group_size = query_count // key_count
    offset = lax.axis_index(EP) * row_count
    score_scale = 1.0 / math.sqrt(HEAD)
    count_rows = queries.shape[0]
    segment_positions = offset + jnp.arange(count_rows, dtype=jnp.int32)
    gate_rows = lax.dynamic_slice_in_dim(forget_cache, offset, count_rows, 1)
    segment_bias = gate_rows.T.reshape(count_rows, key_count, group_size, 1)
    segments = [
        (queries.reshape(count_rows, key_count, group_size, HEAD), segment_positions, segment_bias)
    ]
    start_states = tuple(
        [
            (
                jnp.full((grouped.shape[0], key_count, group_size), -jnp.inf, jnp.float32),
                jnp.zeros((grouped.shape[0], key_count, group_size), jnp.float32),
                jnp.zeros((grouped.shape[0], key_count, group_size, HEAD), jnp.float32),
            )
            for grouped, positions, bias in segments
        ]
    )
    piece_rows = gathered_by_axis(keys_values.reshape(row_count, key_count, 2 * HEAD), EP, 0)
    count_rows = piece_rows.shape[0]
    block_width = 512
    blocks = piece_rows.reshape(count_rows // block_width, block_width, key_count, 2 * HEAD)

    def one_block(states, scan_item):
        block_rows, block_index = scan_item
        first_key = block_index * block_width
        key_block = block_rows[:, :, :HEAD]
        value_block = block_rows[:, :, HEAD:]
        key_gate = lax.dynamic_slice_in_dim(forget_cache, first_key, block_width, 1).reshape(
            1, key_count, group_size, block_width
        )
        key_pos = first_key + jnp.arange(block_width, dtype=jnp.int32)
        updated = []
        for (grouped, positions, bias), state in zip(segments, states):

            def take_block(state_in, grouped=grouped, positions=positions, bias=bias):
                running_max, running_sum, weighted = state_in
                scores = (
                    jnp.einsum(
                        "qhgd,khd->qhgk", grouped, key_block, preferred_element_type=jnp.float32
                    )
                    * score_scale
                )
                scores = scores + bias - key_gate
                visible = (key_pos[None, :] <= positions[:, None])[:, None, None, :]
                scores = jnp.where(visible, scores, -jnp.inf)
                new_max = jnp.maximum(running_max, jnp.max(scores, axis=-1))
                safe_max = jnp.where(jnp.isfinite(new_max), new_max, 0.0)
                factor = jnp.exp(running_max - safe_max)
                weights = jnp.exp(scores - safe_max[..., None])
                running_sum = running_sum * factor + jnp.sum(weights, axis=-1)
                weighted = weighted * factor[..., None] + jnp.einsum(
                    "qhgk,khd->qhgd",
                    weights.astype(jnp.bfloat16),
                    value_block,
                    preferred_element_type=jnp.float32,
                )
                return (new_max, running_sum, weighted)

            def keep_state(state_in):
                return state_in

            updated.append(lax.cond(first_key <= positions[-1], take_block, keep_state, state))
        return (tuple(updated), None)

    final_states, _ = lax.scan(
        one_block, start_states, (blocks, jnp.arange(count_rows // block_width, dtype=jnp.int32))
    )
    outputs = [
        (weighted / running_sum[..., None])
        .reshape(running_sum.shape[0], query_count * HEAD)
        .astype(jnp.bfloat16)
        for running_max, running_sum, weighted in final_states
    ]
    attended = outputs[0]
    local_rows = lax.all_to_all(attended, "tp", split_axis=0, concat_axis=1, tiled=True)
    heads_normed = scaled_rows(local_rows, heads_gain)
    mixer_out = jnp.dot(heads_normed, output_weight, preferred_element_type=jnp.float32).astype(
        jnp.bfloat16
    )
    experts_count = lax.axis_size(EP)
    expert_rows, pick_count = routes.shape
    capacity = 2 * expert_rows * pick_count // experts_count
    expert_in = scaled_rows(expert_tokens, expert_gain)
    shifted = route_logits - jnp.max(route_logits, axis=1, keepdims=True)
    raised = jnp.exp(shifted)
    route_weight = raised / jnp.sum(raised, axis=1, keepdims=True)
    position, slot_token = assign_slots(routes, experts_count, capacity)
    model_width = expert_in.shape[1]
    part_width = model_width // lax.axis_size("tp")
    gate_local = gate_weight[0]
    up_local = up_weight[0]
    down_local = down_weight[0]
    own_columns = lax.dynamic_slice_in_dim(
        expert_in, lax.axis_index("tp") * part_width, part_width, 1
    )
    padded = jnp.concatenate([own_columns, jnp.zeros((1, part_width), jnp.bfloat16)], axis=0)
    outgoing = jnp.take(padded, slot_token, axis=0).reshape(experts_count, capacity, part_width)
    arrived = lax.all_to_all(outgoing, EP, split_axis=0, concat_axis=0, tiled=True).reshape(
        experts_count * capacity, part_width
    )
    piece_rows = lax.all_gather(arrived, "tp", axis=1, tiled=True)
    gate_sum = jnp.dot(piece_rows, gate_local, preferred_element_type=jnp.float32)
    up_sum = jnp.dot(piece_rows, up_local, preferred_element_type=jnp.float32)
    gate_cut = jnp.minimum(gate_sum, clamp_limit)
    up_cut = jnp.clip(up_sum, -clamp_limit, clamp_limit)
    hidden = ((up_cut + 1.0) * gate_cut * jax.nn.sigmoid(sigmoid_slope * gate_cut)).astype(
        jnp.bfloat16
    )
    expert_out = sent_and_summed(
        lax.dot_general(
            down_local, hidden, (((0,), (1,)), ((), ())), preferred_element_type=jnp.float32
        ).astype(jnp.bfloat16),
        "tp",
        0,
    ).astype(jnp.bfloat16)
    returned = lax.all_to_all(expert_out, EP, split_axis=1, concat_axis=1, tiled=True)
    picked = jnp.take(returned, position.reshape(-1), axis=1).reshape(
        part_width, expert_rows, pick_count
    )
    moe_out = jnp.einsum("crk,rk->rc", picked.astype(jnp.float32), route_weight).astype(
        jnp.bfloat16
    )
    return (mixer_out, moe_out)


def solution(mesh):
    torus = Mesh(mesh.devices.reshape(8, 4, mesh.shape["tp"]), ("ep_0", "ep_1", "tp"))
    return jax.shard_map(
        body,
        mesh=torus,
        in_specs=(
            P(EP, "tp"),
            P(EP, "tp"),
            P("tp", None),
            P(),
            P(),
            P(EP, None),
            P(),
            P(EP, None),
            P(EP, None),
            P(EP, None, "tp"),
            P(EP, None, "tp"),
            P(EP, "tp", None),
        ),
        out_specs=(P(EP_TP, None), P(EP, "tp")),
        check_vma=False,
    )
```

profile of v0, /device:TPU:2, one launch (start us, length us, event | category | flops | bytes accessed | tf_op | source)
XLA Modules:
  0.0 385.4 jit_solution(9211881118816011675)
XLA Ops:
  7.2 1.2 convert_element_type.73
  8.4 1.2 multiply_reduce_fusion
  11.4 1.2 reduce-window.6
  13.2 2.4 scatter_custom_fusion
  16.6 3.9 %gather_fusion = bf16[1024,256]{1,0:T(8,128)(2,1)S(1)} fusion(bf16[129,256]{1,0:T(8,128)(2,1)S(1)} %concatenate.3, s32[1024]{0:T(1024)S(1)} %fusion.43), kind=kCustom, calls=%fused_computation | custom fusion | bytes 1052672 | tf_op jit(solution)/shard_map/jit(_take)/gather | solution.py:170
  20.8 28.3 %all_to_all.32 = bf16[32,32,256]{2,1,0:T(8,128)(2,1)} all-to-all(bf16[32,32,256]{2,1,0:T(8,128)(2,1)S(1)} %broadcast_select_fusion), channel_id=1, replica_groups=mesh['ep_0'=8,'ep_1'=4,'tp'=8] {'ep_0','ep_1'}, dimensions={0} | all-to-all | bytes 1048576 | tf_op jit(solution)/shard_map/all_to_all | solution.py:171
  49.2 13.8 %all-gather = bf16[2048,128]{1,0:T(8,128)(2,1)} all-gather(bf16[512,128]{1,0:T(8,128)(2,1)S(1)} %copy-done.1), channel_id=2, replica_groups=mesh['ep_0'=8,'ep_1'=4,'tp'=8] {'ep_1'}, dimensions={0}, use_global_device_ids=true | all-gather | bytes 655360 | tf_op jit(solution)/shard_map/all_gather | solution.py:19
  63.1 21.2 %all-gather.5.cloned.1.call-done = bf16[1024,2048]{1,0:T(8,128)(2,1)} async-done(((bf16[1024,256]{1,0:T(8,128)(2,1)}), bf16[1024,2048]{1,0:T(8,128)(2,1)}) %all-gather.5.cloned.1.call-update) | async-done | bytes 4194320 | tf_op jit(solution)/shard_map/all_gather | solution.py:174
  84.3 4.5 %convolution_minimum_fusion = f32[1024,256]{1,0:T(8,128)} fusion(bf16[1024,2048]{1,0:T(8,128)(2,1)} %all-gather.5.cloned.1.call-done, bf16[1,2048,256]{2,1,0:T(8,128)(2,1)S(1)} %copy-done.6), kind=kOutput, calls=%fused_computation.29 | convolution fusion | flops 1074003968 | bytes 6291456 | tf_op jit(solution)/shard_map/dot_general | solution.py:175
  88.8 8.8 %convolution_convert_fusion = bf16[1024,2048]{1,0:T(8,128)(2,1)} fusion(f32[1024,256]{1,0:T(8,128)} %convolution_minimum_fusion, bf16[1024,2048]{1,0:T(8,128)(2,1)} %all-gather.5.cloned.1.call-done, bf16[1,256,2048]{2,1,0:T(8,128)(2,1)S(1)} %copy-done, bf16[1,2048,256]{2,1,0:T(8,128)(2,1)S(1)} %copy-done.7), kind=kOutput, calls=%fused_computation.27 | convolution fusion | flops 2151940096 | bytes 11534336 | tf_op jit(solution)/shard_map/dot_general | solution.py:183
  97.7 4.6 %copy.58 = bf16[128,8,8,256]{3,2,0,1:T(8,128)(2,1)} copy(bf16[128,8,8,256]{3,2,1,0:T(8,128)(2,1)} %bitcast.128) | data formatting | bytes 8388608 | tf_op jit(solution)/shard_map/reshape | solution.py:25
  102.3 4.7 %all-to-all-start.2 = ((bf16[8,256,1024]{1,2,0:T(8,128)(2,1)}), bf16[8,256,1024]{1,2,0:T(8,128)(2,1)}, u32[]{:S(2)}, u32[]{:S(2)}) async-start(bf16[8,256,1024]{1,2,0:T(8,128)(2,1)} %bitcast.125), calls=%async_computation.2 | async-start | bytes 8388608 | tf_op jit(solution)/shard_map/all_to_all | solution.py:30
  108.0 33.8 %all-gather.7.cloned.1.call-done = bf16[16384,128]{1,0:T(8,128)(2,1)} async-done(((bf16[2048,128]{1,0:T(8,128)(2,1)}), bf16[16384,128]{1,0:T(8,128)(2,1)}) %all-gather.7.cloned.1.call-update) | async-done | bytes 4194320 | tf_op jit(solution)/shard_map/all_gather | solution.py:19
  141.8 6.5 %copy.37 = bf16[32,512,1,128]{1,3,2,0:T(8,128)(2,1)} copy(bf16[32,512,1,128]{3,1,0,2:T(8,128)(2,1)} %bitcast.127) | data formatting | bytes 8388608 | tf_op jit(solution)/shard_map/while | solution.py:138
  148.4 87.1 %while.14 = (s32[]{:T(128)}, f32[512,1,2]{0,2,1:T(2,128)S(1)}, f32[512,1,2]{0,2,1:T(2,128)S(1)}, f32[512,1,2,64]{0,3,2,1:T(8,128)S(1)}, s32[32]{0:T(128)S(1)}, /...) while((s32[]{:T(128)}, f32[512,1,2]{0,2,1:T(2,128)S(1)}, ...), condition=%wide.region_5.6_spmd, body=%wide.region_0.5_spmd.sunk | while | flops 139339264 | bytes 7965025 | solution.py:138
  150.9 3.6 conditional.2
  156.9 3.6 conditional.2
  236.6 4.3 %all-to-all-start = ((bf16[8,64,128]{2,1,0:T(8,128)(2,1)}), bf16[8,64,128]{2,1,0:T(8,128)(2,1)S(1)}, u32[]{:S(2)}, u32[]{:S(2)}) async-start(bf16[8,64,128]{2,1,0:T(8,128)(2,1)} %copy.38), calls=%async_computation | async-start | bytes 262144 | tf_op jit(solution)/shard_map/all_to_all | solution.py:148
  241.1 3.7 reduce_sum.68
  244.8 2.2 all-to-all-done
  247.0 111.8 %all-to-all-start.3 = ((bf16[256,32,32]{0,2,1:T(8,128)(2,1)}), bf16[256,32,32]{0,2,1:T(8,128)(2,1)S(1)}, u32[]{:S(2)}, u32[]{:S(2)}) async-start(bf16[256,32,32]{0,2,1:T(8,128)(2,1)} %bitcast.33), calls=%async_computation.3 | async-start | bytes 1048576 | tf_op jit(solution)/shard_map/all_to_all | solution.py:189
  359.2 3.8 convolution_convert_fusion.1
  363.0 12.5 %all-to-all-done.3 = bf16[256,32,32]{0,2,1:T(8,128)(2,1)S(1)} async-done(((bf16[256,32,32]{0,2,1:T(8,128)(2,1)}), bf16[256,32,32]{0,2,1:T(8,128)(2,1)S(1)}, u32[]{:S(2)}, u32[]{:S(2)}) %all-to-all-start.3) | async-done | bytes 524320 | tf_op jit(solution)/shard_map/all_to_all | solution.py:189
  375.5 1.9 gather_fusion.1
  (214 shorter events, 52.3 us)
Async XLA Ops:
  7.2 81.7 %copy-start = (bf16[1,256,2048]{2,1,0:T(8,128)(2,1)S(1)}, bf16[1,256,2048]{2,1,0:T(8,128)(2,1)}, u32[]{:S(2)}) copy-start(bf16[1,256,2048]{2,1,0:T(8,128)(2,1)} %param.27) | copy-start | bytes 3145732
  7.2 77.1 %all-gather.5.cloned.1.call-start = ((), (), s32[]{:S(2)}) async-start(), calls=%async_computation.4 | async-start | bytes 4718592 | tf_op jit(solution)/shard_map/all_gather | solution.py:174
  10.5 38.8 %copy-start.1 = (bf16[512,128]{1,0:T(8,128)(2,1)S(1)}, bf16[512,128]{1,0:T(8,128)(2,1)}, u32[]{:S(2)}) copy-start(bf16[512,128]{1,0:T(8,128)(2,1)} %param.17) | copy-start | bytes 393220
  16.6 67.7 %copy-start.6 = (bf16[1,2048,256]{2,1,0:T(8,128)(2,1)S(1)}, bf16[1,2048,256]{2,1,0:T(8,128)(2,1)}, u32[]{:S(2)}) copy-start(bf16[1,2048,256]{2,1,0:T(8,128)(2,1)} %param.25) | copy-start | bytes 3145732
  49.2 39.7 %copy-start.7 = (bf16[1,2048,256]{2,1,0:T(8,128)(2,1)S(1)}, bf16[1,2048,256]{2,1,0:T(8,128)(2,1)}, u32[]{:S(2)}) copy-start(bf16[1,2048,256]{2,1,0:T(8,128)(2,1)} %param.26) | copy-start | bytes 3145732
  49.2 92.7 %all-gather.7.cloned.1.call-start = ((), (), s32[]{:S(2)}) async-start(), calls=%async_computation.5 | async-start | bytes 4718592 | tf_op jit(solution)/shard_map/all_gather | solution.py:19
  102.3 4.8 %copy-start.2 = (bf16[512,128]{1,0:T(8,128)(2,1)S(1)}, bf16[512,128]{1,0:T(8,128)(2,1)}, u32[]{:S(2)}) copy-start(bf16[512,128]{1,0:T(8,128)(2,1)} %param.16) | copy-start | bytes 393220
  102.3 134.3 %all-to-all-start.2 = ((bf16[8,256,1024]{1,2,0:T(8,128)(2,1)}), bf16[8,256,1024]{1,2,0:T(8,128)(2,1)}, u32[]{:S(2)}, u32[]{:S(2)}) async-start(bf16[8,256,1024]{1,2,0:T(8,128)(2,1)} %bitcast.125), calls=%async_computation.2 | async-start | bytes 8388608 | tf_op jit(solution)/shard_map/all_to_all | solution.py:30
  148.4 92.5 %copy-start.3 = (s32[128,4]{0,1:T(4,128)S(1)}, s32[128,4]{0,1:T(4,128)}, u32[]{:S(2)}) copy-start(s32[128,4]{0,1:T(4,128)} %param.23) | copy-start | bytes 6148
  148.4 92.7 %copy-start.4 = (f32[128,4]{0,1:T(4,128)S(1)}, f32[128,4]{0,1:T(4,128)}, u32[]{:S(2)}) copy-start(f32[128,4]{0,1:T(4,128)} %param.24) | copy-start | bytes 6148
  235.5 123.6 %copy-start.5 = (f32[1024]{0:T(1024)S(1)}, f32[1024]{0:T(1024)}, u32[]{:S(2)}) copy-start(f32[1024]{0:T(1024)} %param.19) | copy-start | bytes 12292
  236.6 10.4 %all-to-all-start = ((bf16[8,64,128]{2,1,0:T(8,128)(2,1)}), bf16[8,64,128]{2,1,0:T(8,128)(2,1)S(1)}, u32[]{:S(2)}, u32[]{:S(2)}) async-start(bf16[8,64,128]{2,1,0:T(8,128)(2,1)} %copy.38), calls=%async_computation | async-start | bytes 262144 | tf_op jit(solution)/shard_map/all_to_all | solution.py:148
  247.0 128.5 %all-to-all-start.3 = ((bf16[256,32,32]{0,2,1:T(8,128)(2,1)}), bf16[256,32,32]{0,2,1:T(8,128)(2,1)S(1)}, u32[]{:S(2)}, u32[]{:S(2)}) async-start(bf16[256,32,32]{0,2,1:T(8,128)(2,1)} %bitcast.33), calls=%async_computation.3 | async-start | bytes 1048576 | tf_op jit(solution)/shard_map/all_to_all | solution.py:189
Sparse Core Ops, SparseCore 0:
  49.3 34.9 all-gather.4
  86.1 55.6 all-gather.6
where the time goes:
time: 388 us; the launch traced here: 385 us
  starting transfers between devices  121 us (31%)
  waiting for transfers between devices  69.8 us (18%)
  local copies, waits for them, and re-layouts  65.9 us (17%)
  loops' own time  42.4 us (11%)
  blocking collectives  42.2 us (11%)
  matrix products  20 us (5%)
  between operations  14.3 us (4%)
  other arithmetic  9.81 us (3%)
    all_to_all x1, starting transfers between devices, body(): lax.all_to_all(expert_out, EP, split_axis=1, concat_axis=1, tiled=True)  112 us
    another operation x1, loops' own time, body(): lax.scan(one_block, start_states, (blocks, jnp.arange(count_rows // block...  41.9 us
    all_gather x1, waiting for transfers between devices, gathered_by_axis(): whole = lax.all_gather(whole, axes[number], axis=dim, tiled=True)  33.8 us
    all_to_all x1, blocking collectives, body(): lax.all_to_all(outgoing, EP, split_axis=0, concat_axis=0, tiled=True)  28.3 us
    all_gather x1, waiting for transfers between devices, body(): piece_rows = lax.all_gather(arrived, 'tp', axis=1, tiled=True)  21.2 us
    slice x32, local copies, waits for them, and re-layouts, one_block(): positions[-1]  18.9 us
    dynamic_slice x32, local copies, waits for them, and re-layouts, body(): lax.scan(one_block, start_states, (blocks, jnp.arange(count_rows // block...  18.8 us
    all_gather x1, blocking collectives, gathered_by_axis(): whole = lax.all_gather(whole, axes[number], axis=dim, tiled=True)  13.8 us
  transfers between devices with their start and end apart: 5, of which 4 were waited for; matrix products, arithmetic and copies ran while one was open for 21% of the time, Pallas kernels for 0%

commit v1 on v0

--- a/solution.py
+++ b/solution.py
@@ -11,6 +11,22 @@
 epsilon = 1e-06
 clamp_limit = 7.0
 sigmoid_slope = 1.702
+
+
+def collect(x, axis, dim):
+    ways, here, hop = (lax.axis_size(axis), lax.axis_index(axis), x.shape[dim])
+    dims = [n * ways if d == dim else n for d, n in enumerate(x.shape)]
+    full = lax.dynamic_update_slice_in_dim(jnp.zeros(dims, x.dtype), x, here * hop, axis=dim)
+    going_up = going_down = x
+    for far in range(1, ways // 2 + 1):
+        going_up = lax.ppermute(going_up, axis, [(d, (d + 1) % ways) for d in range(ways)])
+        full = lax.dynamic_update_slice_in_dim(full, going_up, (here - far) % ways * hop, axis=dim)
+        if 2 * far < ways:
+            going_down = lax.ppermute(going_down, axis, [(d, (d - 1) % ways) for d in range(ways)])
+            full = lax.dynamic_update_slice_in_dim(
+                full, going_down, (here + far) % ways * hop, axis=dim
+            )
+    return full
 
 
 def gathered_by_axis(array, axes, dim):
@@ -171,7 +187,7 @@
     arrived = lax.all_to_all(outgoing, EP, split_axis=0, concat_axis=0, tiled=True).reshape(
         experts_count * capacity, part_width
     )
-    piece_rows = lax.all_gather(arrived, "tp", axis=1, tiled=True)
+    piece_rows = collect(arrived, "tp", 1)
     gate_sum = jnp.dot(piece_rows, gate_local, preferred_element_type=jnp.float32)
     up_sum = jnp.dot(piece_rows, up_local, preferred_element_type=jnp.float32)
     gate_cut = jnp.minimum(gate_sum, clamp_limit)

time: 388 us -> 357 us (0.920)
  blocking collectives: 42.2 us -> 15.8 us
  waiting for transfers between devices: 69.8 us -> 44.2 us
  starting transfers between devices: 121 us -> 142 us
    all_gather x1, waiting for transfers between devices: 33.8 us -> 0.01 us  [gathered_by_axis(): whole = lax.all_gather(whole, axes[number], axis=dim, tiled=True)]
    ppermute x0 -> x7, waiting for transfers between devices: none -> 28.6 us  [the longest x4 28.6 us: collect(): lax.ppermute(going_up, axis, [(d, (d + 1) % ways) for d in range(ways)])]
    all_to_all x1 -> x0, blocking collectives: 28.3 us -> none  [body(): lax.all_to_all(outgoing, EP, split_axis=0, concat_axis=0, tiled=True)]
    all_gather x1 -> x0, waiting for transfers between devices: 21.2 us -> none  [body(): piece_rows = lax.all_gather(arrived, 'tp', axis=1, tiled=True)]
    all_to_all x0 -> x1, starting transfers between devices: none -> 11.6 us  [body(): lax.all_to_all(outgoing, EP, split_axis=0, concat_axis=0, tiled=True)]
    ppermute x0 -> x7, starting transfers between devices: none -> 8.88 us  [the longest x3 8.87 us: collect(): lax.ppermute(going_down, axis, [(d, (d - 1) % ways) for d in range(ways)])]
  transfers between devices with their start and end apart: 5 -> 12, of which waited for: 4 -> 7; matrix products, arithmetic and copies ran while one was open for 21% -> 22% of each run, Pallas kernels for 0% -> 0%
where the time goes in v1:
time: 357 us; the launch traced here: 354 us
  starting transfers between devices  142 us (40%)
  local copies, waits for them, and re-layouts  69.3 us (19%)
  waiting for transfers between devices  44.2 us (12%)
  loops' own time  40.6 us (11%)
  matrix products  16.5 us (5%)
  blocking collectives  15.8 us (4%)
  between operations  14.5 us (4%)
  other arithmetic  10.6 us (3%)
    all_to_all x1, starting transfers between devices, body(): lax.all_to_all(expert_out, EP, split_axis=1, concat_axis=1, tiled=True)  112 us
    another operation x1, loops' own time, body(): lax.scan(one_block, start_states, (blocks, jnp.arange(count_rows // block...  40 us
    ppermute x4, waiting for transfers between devices, collect(): lax.ppermute(going_up, axis, [(d, (d + 1) % ways) for d in range(ways)])  28.6 us
    dynamic_slice x32, local copies, waits for them, and re-layouts, body(): lax.scan(one_block, start_states, (blocks, jnp.arange(count_rows // block...  18.8 us
    slice x32, local copies, waits for them, and re-layouts, one_block(): positions[-1]  18.4 us
    all_gather x1, blocking collectives, gathered_by_axis(): whole = lax.all_gather(whole, axes[number], axis=dim, tiled=True)  15.8 us
    all_to_all x1, waiting for transfers between devices, body(): lax.all_to_all(expert_out, EP, split_axis=1, concat_axis=1, tiled=True)  12.5 us
    all_to_all x1, starting transfers between devices, body(): lax.all_to_all(outgoing, EP, split_axis=0, concat_axis=0, tiled=True)  11.6 us
  transfers between devices with their start and end apart: 12, of which 7 were waited for; matrix products, arithmetic and copies ran while one was open for 22% of the time, Pallas kernels for 0%

profile of v1, /device:TPU:2, one launch (start us, length us, event | category | flops | bytes accessed | tf_op | source)
XLA Modules:
  0.0 353.8 jit_solution(8555545510241620625)
XLA Ops:
  13.2 2.4 scatter_custom_fusion
  16.6 3.9 %gather_fusion = bf16[1024,256]{1,0:T(8,128)(2,1)S(1)} fusion(bf16[129,256]{1,0:T(8,128)(2,1)S(1)} %concatenate.3, s32[1024]{0:T(1024)S(1)} %fusion.43), kind=kCustom, calls=%fused_computation | custom fusion | bytes 1052672 | tf_op jit(solution)/shard_map/jit(_take)/gather | solution.py:186
  21.6 11.6 %all-to-all-start.1 = ((bf16[32,32,256]{2,1,0:T(8,128)(2,1)}), bf16[32,32,256]{2,1,0:T(8,128)(2,1)S(1)}, u32[]{:S(2)}, u32[]{:S(2)}) async-start(bf16[32,32,256]{2,1,0:T(8,128)(2,1)} %broadcast_select_fusion), calls=%async_computation.1 | async-start | bytes 1048576 | tf_op jit(solution)/shard_map/all_to_all | solution.py:187
  33.3 15.8 %all-gather = bf16[2048,128]{1,0:T(8,128)(2,1)} all-gather(bf16[512,128]{1,0:T(8,128)(2,1)S(1)} %copy-done.4), channel_id=2, replica_groups=mesh['ep_0'=8,'ep_1'=4,'tp'=8] {'ep_1'}, dimensions={0}, use_global_device_ids=true | all-gather | bytes 655360 | tf_op jit(solution)/shard_map/all_gather | solution.py:35
  50.0 3.0 collective-permute-start.1
  53.0 6.9 %collective-permute-done = bf16[1024,256]{1,0:T(8,128)(2,1)S(1)} collective-permute-done((bf16[1024,256]{1,0:T(8,128)(2,1)S(1)}, bf16[1024,256]{1,0:T(8,128)(2,1)S(1)}, u32[]{:S(2)}, u32[]{:S(2)}) %collective-permute-start) | collective-permute-done | bytes 524320 | tf_op jit(solution)/shard_map/ppermute | solution.py:22
  59.9 3.0 collective-permute-start.3
  62.8 7.0 %collective-permute-done.2 = bf16[1024,256]{1,0:T(8,128)(2,1)} collective-permute-done((bf16[1024,256]{1,0:T(8,128)(2,1)S(1)}, bf16[1024,256]{1,0:T(8,128)(2,1)}, u32[]{:S(2)}, u32[]{:S(2)}) %collective-permute-start.2) | collective-permute-done | bytes 524320 | tf_op jit(solution)/shard_map/ppermute | solution.py:22
  70.4 3.0 collective-permute-start.5
  73.4 6.4 %collective-permute-done.4 = bf16[1024,256]{1,0:T(8,128)(2,1)S(1)} collective-permute-done((bf16[1024,256]{1,0:T(8,128)(2,1)}, bf16[1024,256]{1,0:T(8,128)(2,1)S(1)}, u32[]{:S(2)}, u32[]{:S(2)}) %collective-permute-start.4) | collective-permute-done | bytes 524320 | tf_op jit(solution)/shard_map/ppermute | solution.py:22
  81.2 8.4 %collective-permute-done.6 = bf16[1024,256]{1,0:T(8,128)(2,1)S(1)} collective-permute-done((bf16[1024,256]{1,0:T(8,128)(2,1)S(1)}, bf16[1024,256]{1,0:T(8,128)(2,1)S(1)}, u32[]{:S(2)}, u32[]{:S(2)}) %collective-permute-start.6) | collective-permute-done | bytes 524320 | tf_op jit(solution)/shard_map/ppermute | solution.py:22
  92.9 8.6 %convolution_convert_fusion = bf16[1024,2048]{1,0:T(8,128)(2,1)} fusion(f32[1024,256]{1,0:T(8,128)S(1)} %convolution_minimum_fusion, bf16[1024,2048]{1,0:T(8,128)(2,1)} %copy-done.1, bf16[1,256,2048]{2,1,0:T(8,128)(2,1)S(1)} %copy-done, bf16[1,2048,256]{2,1,0:T(8,128)(2,1)S(1)} %copy-done.10), kind=kOutput, calls=%fused_computation.27 | convolution fusion | flops 2151940096 | bytes 11534336 | tf_op jit(solution)/shard_map/dot_general | solution.py:199
  101.5 4.4 %copy.58 = bf16[128,8,8,256]{3,2,0,1:T(8,128)(2,1)} copy(bf16[128,8,8,256]{3,2,1,0:T(8,128)(2,1)} %bitcast.128) | data formatting | bytes 8388608 | tf_op jit(solution)/shard_map/reshape | solution.py:41
  106.0 4.7 %all-to-all-start.2 = ((bf16[8,256,1024]{1,2,0:T(8,128)(2,1)}), bf16[8,256,1024]{1,2,0:T(8,128)(2,1)}, u32[]{:S(2)}, u32[]{:S(2)}) async-start(bf16[8,256,1024]{1,2,0:T(8,128)(2,1)} %bitcast.125), calls=%async_computation.2 | async-start | bytes 8388608 | tf_op jit(solution)/shard_map/all_to_all | solution.py:46
  111.7 6.5 %copy.37 = bf16[32,512,1,128]{1,3,2,0:T(8,128)(2,1)} copy(bf16[32,512,1,128]{3,1,0,2:T(8,128)(2,1)} %bitcast.127) | data formatting | bytes 8388608 | tf_op jit(solution)/shard_map/while | solution.py:154
  118.2 84.8 %while.14 = (s32[]{:T(128)}, f32[512,1,2]{0,2,1:T(2,128)S(1)}, f32[512,1,2]{0,2,1:T(2,128)S(1)}, f32[512,1,2,64]{0,3,2,1:T(8,128)S(1)}, s32[32]{0:T(128)S(1)}, /...) while((s32[]{:T(128)}, f32[512,1,2]{0,2,1:T(2,128)S(1)}, ...), condition=%wide.region_5.6_spmd, body=%wide.region_0.5_spmd.sunk | while | flops 139339264 | bytes 7965025 | solution.py:154
  120.7 3.6 %conditional.2 = ((f32[512,1,2]{0,2,1:T(2,128)S(1)}, f32[512,1,2]{0,2,1:T(2,128)S(1)}, f32[512,1,2,64]{0,3,2,1:T(8,128)S(1)})) conditional(s32[]{:T(128)} %convert_element_type.105, (f32[512,1,2]{0,2,1:T(2,128)S(1)}, f32[512,1,2]{0,2,1:T(2,128)S(1)}, f32[512,1,2,64]{0,3,2,1:T(8,128)S(1)}) %tuple.45, (s32[]{:T(128)}, s32[512]{0:T(512)S(1)}, ...), branch_computations={%region_1.1_spmd, %region_2.4_spmd} | conditional | flops 139339264 | bytes 7962702 | solution.py:151
  126.6 3.6 %conditional.2 = ((f32[512,1,2]{0,2,1:T(2,128)S(1)}, f32[512,1,2]{0,2,1:T(2,128)S(1)}, f32[512,1,2,64]{0,3,2,1:T(8,128)S(1)})) conditional(s32[]{:T(128)} %convert_element_type.105, (f32[512,1,2]{0,2,1:T(2,128)S(1)}, f32[512,1,2]{0,2,1:T(2,128)S(1)}, f32[512,1,2,64]{0,3,2,1:T(8,128)S(1)}) %tuple.45, (s32[]{:T(128)}, s32[512]{0:T(512)S(1)}, ...), branch_computations={%region_1.1_spmd, %region_2.4_spmd} | conditional | flops 139339264 | bytes 7962702 | solution.py:151
  204.2 4.7 %all-to-all-start = ((bf16[8,64,128]{2,1,0:T(8,128)(2,1)}), bf16[8,64,128]{2,1,0:T(8,128)(2,1)S(1)}, u32[]{:S(2)}, u32[]{:S(2)}) async-start(bf16[8,64,128]{2,1,0:T(8,128)(2,1)} %copy.38), calls=%async_computation | async-start | bytes 262144 | tf_op jit(solution)/shard_map/all_to_all | solution.py:164
  209.1 3.7 %reduce_sum.68 = bf16[256,1024]{0,1:T(8,128)(2,1)} reduce(bf16[8,256,1024]{1,2,0:T(8,128)(2,1)} %all-to-all-done.2, bf16[]{:T(256)} %constant.174.clone.1), dimensions={0}, to_apply=%region_12.13 | reduce | flops 1835008 | bytes 4718594 | tf_op jit(solution)/shard_map/reduce_sum | solution.py:47
  212.7 2.2 all-to-all-done
  214.9 112.4 %all-to-all-start.3 = ((bf16[256,32,32]{0,2,1:T(8,128)(2,1)}), bf16[256,32,32]{0,2,1:T(8,128)(2,1)S(1)}, u32[]{:S(2)}, u32[]{:S(2)}) async-start(bf16[256,32,32]{0,2,1:T(8,128)(2,1)} %bitcast.33), calls=%async_computation.3 | async-start | bytes 1048576 | tf_op jit(solution)/shard_map/all_to_all | solution.py:205
  327.6 3.8 %convolution_convert_fusion.1 = bf16[64,2048]{1,0:T(8,128)(2,1)} fusion(bf16[1024,2048]{1,0:T(8,128)(2,1)} %param.20, f32[1024]{0:T(1024)S(1)} %copy-done.8, f32[64]{0:T(128)S(1)} %add_rsqrt_fusion.1, bf16[8,64,128]{2,1,0:T(8,128)(2,1)S(1)} %all-to-all-done), kind=kOutput, calls=%fused_computation.28 | convolution fusion | flops 268828672 | bytes 4591872 | tf_op jit(solution)/shard_map/dot_general | solution.py:166
  331.4 12.5 %all-to-all-done.3 = bf16[256,32,32]{0,2,1:T(8,128)(2,1)S(1)} async-done(((bf16[256,32,32]{0,2,1:T(8,128)(2,1)}), bf16[256,32,32]{0,2,1:T(8,128)(2,1)S(1)}, u32[]{:S(2)}, u32[]{:S(2)}) %all-to-all-start.3) | async-done | bytes 524320 | tf_op jit(solution)/shard_map/all_to_all | solution.py:205
  (241 shorter events, 64.5 us)
Async XLA Ops:
  7.2 85.8 %copy-start = (bf16[1,256,2048]{2,1,0:T(8,128)(2,1)S(1)}, bf16[1,256,2048]{2,1,0:T(8,128)(2,1)}, u32[]{:S(2)}) copy-start(bf16[1,256,2048]{2,1,0:T(8,128)(2,1)} %param.27) | copy-start | bytes 3145732
  8.4 24.8 %copy-start.4 = (bf16[512,128]{1,0:T(8,128)(2,1)S(1)}, bf16[512,128]{1,0:T(8,128)(2,1)}, u32[]{:S(2)}) copy-start(bf16[512,128]{1,0:T(8,128)(2,1)} %param.17) | copy-start | bytes 393220
  21.6 28.5 %all-to-all-start.1 = ((bf16[32,32,256]{2,1,0:T(8,128)(2,1)}), bf16[32,32,256]{2,1,0:T(8,128)(2,1)S(1)}, u32[]{:S(2)}, u32[]{:S(2)}) async-start(bf16[32,32,256]{2,1,0:T(8,128)(2,1)} %broadcast_select_fusion), calls=%async_computation.1 | async-start | bytes 1048576 | tf_op jit(solution)/shard_map/all_to_all | solution.py:187
  33.2 78.5 %all-gather.4.cloned.1.call-start = ((), (), s32[]{:S(2)}) async-start(), calls=%async_computation.4 | async-start | bytes 4718592 | tf_op jit(solution)/shard_map/all_gather | solution.py:35
  50.0 9.8 %collective-permute-start = (bf16[1024,256]{1,0:T(8,128)(2,1)S(1)}, bf16[1024,256]{1,0:T(8,128)(2,1)S(1)}, u32[]{:S(2)}, u32[]{:S(2)}) collective-permute-start(bf16[1024,256]{1,0:T(8,128)(2,1)S(1)} %bitcast.129), channel_id=1, source_target_pairs={{0,1},{1,2},{2,3},{3,4},{4,5},{5,6},{6,7},{7,0},{8,9},{9,10},{10,1... | collective-permute-start | bytes 1572872 | tf_op jit(solution)/shard_map/ppermute | solution.py:22
  50.0 9.8 %collective-permute-start.1 = (bf16[1024,256]{1,0:T(8,128)(2,1)S(1)}, bf16[1024,256]{1,0:T(8,128)(2,1)S(1)}, u32[]{:S(2)}, u32[]{:S(2)}) collective-permute-start(bf16[1024,256]{1,0:T(8,128)(2,1)S(1)} %bitcast.130), channel_id=1, source_target_pairs={{0,7},{1,0},{2,1},{3,2},{4,3},{5,4},{6,5},{7,6},{8,15},{9,8},{10,9... | collective-permute-start | bytes 1572872 | tf_op jit(solution)/shard_map/ppermute | solution.py:25
  59.8 3.0 copy-start.2
  59.8 9.9 %collective-permute-start.2 = (bf16[1024,256]{1,0:T(8,128)(2,1)S(1)}, bf16[1024,256]{1,0:T(8,128)(2,1)}, u32[]{:S(2)}, u32[]{:S(2)}) collective-permute-start(bf16[1024,256]{1,0:T(8,128)(2,1)S(1)} %collective-permute-done), channel_id=1, source_target_pairs={{0,1},{1,2},{2,3},{3,4},{4,5},{5,6},{6,7},{7,0},{8,9},{9,10},{10,1... | collective-permute-start | bytes 1572872 | tf_op jit(solution)/shard_map/ppermute | solution.py:22
  59.9 10.5 %collective-permute-start.3 = (bf16[1024,256]{1,0:T(8,128)(2,1)S(1)}, bf16[1024,256]{1,0:T(8,128)(2,1)S(1)}, u32[]{:S(2)}, u32[]{:S(2)}) collective-permute-start(bf16[1024,256]{1,0:T(8,128)(2,1)S(1)} %collective-permute-done.1), channel_id=1, source_target_pairs={{0,7},{1,0},{2,1},{3,2},{4,3},{5,4},{6,5},{7,6},{8,15},{9,8},{10,9... | collective-permute-start | bytes 1572872 | tf_op jit(solution)/shard_map/ppermute | solution.py:25
  69.8 10.0 %collective-permute-start.4 = (bf16[1024,256]{1,0:T(8,128)(2,1)}, bf16[1024,256]{1,0:T(8,128)(2,1)S(1)}, u32[]{:S(2)}, u32[]{:S(2)}) collective-permute-start(bf16[1024,256]{1,0:T(8,128)(2,1)} %collective-permute-done.2), channel_id=1, source_target_pairs={{0,1},{1,2},{2,3},{3,4},{4,5},{5,6},{6,7},{7,0},{8,9},{9,10},{10,1... | collective-permute-start | bytes 1572872 | tf_op jit(solution)/shard_map/ppermute | solution.py:22
  69.8 3.6 %copy-start.3 = (bf16[1024,256]{1,0:T(8,128)(2,1)S(1)}, bf16[1024,256]{1,0:T(8,128)(2,1)}, u32[]{:S(2)}) copy-start(bf16[1024,256]{1,0:T(8,128)(2,1)} %copy-done.2) | copy-start | bytes 1572868
  70.3 21.4 %copy-start.9 = (bf16[1,2048,256]{2,1,0:T(8,128)(2,1)S(1)}, bf16[1,2048,256]{2,1,0:T(8,128)(2,1)}, u32[]{:S(2)}) copy-start(bf16[1,2048,256]{2,1,0:T(8,128)(2,1)} %param.25) | copy-start | bytes 3145732
  70.4 10.8 %collective-permute-start.5 = (bf16[1024,256]{1,0:T(8,128)(2,1)S(1)}, bf16[1024,256]{1,0:T(8,128)(2,1)S(1)}, u32[]{:S(2)}, u32[]{:S(2)}) collective-permute-start(bf16[1024,256]{1,0:T(8,128)(2,1)S(1)} %collective-permute-done.3), channel_id=1, source_target_pairs={{0,7},{1,0},{2,1},{3,2},{4,3},{5,4},{6,5},{7,6},{8,15},{9,8},{10,9... | collective-permute-start | bytes 1572872 | tf_op jit(solution)/shard_map/ppermute | solution.py:25
  79.8 9.8 %collective-permute-start.6 = (bf16[1024,256]{1,0:T(8,128)(2,1)S(1)}, bf16[1024,256]{1,0:T(8,128)(2,1)S(1)}, u32[]{:S(2)}, u32[]{:S(2)}) collective-permute-start(bf16[1024,256]{1,0:T(8,128)(2,1)S(1)} %collective-permute-done.4), channel_id=1, source_target_pairs={{0,1},{1,2},{2,3},{3,4},{4,5},{5,6},{6,7},{7,0},{8,9},{9,10},{10,1... | collective-permute-start | bytes 1572872 | tf_op jit(solution)/shard_map/ppermute | solution.py:22
  81.2 11.7 %copy-start.10 = (bf16[1,2048,256]{2,1,0:T(8,128)(2,1)S(1)}, bf16[1,2048,256]{2,1,0:T(8,128)(2,1)}, u32[]{:S(2)}) copy-start(bf16[1,2048,256]{2,1,0:T(8,128)(2,1)} %param.26) | copy-start | bytes 3145732
  89.7 2.0 copy-start.1
  106.0 4.9 %copy-start.5 = (bf16[512,128]{1,0:T(8,128)(2,1)S(1)}, bf16[512,128]{1,0:T(8,128)(2,1)}, u32[]{:S(2)}) copy-start(bf16[512,128]{1,0:T(8,128)(2,1)} %param.16) | copy-start | bytes 393220
  106.0 98.2 %all-to-all-start.2 = ((bf16[8,256,1024]{1,2,0:T(8,128)(2,1)}), bf16[8,256,1024]{1,2,0:T(8,128)(2,1)}, u32[]{:S(2)}, u32[]{:S(2)}) async-start(bf16[8,256,1024]{1,2,0:T(8,128)(2,1)} %bitcast.125), calls=%async_computation.2 | async-start | bytes 8388608 | tf_op jit(solution)/shard_map/all_to_all | solution.py:46
  118.2 90.6 %copy-start.6 = (s32[128,4]{0,1:T(4,128)S(1)}, s32[128,4]{0,1:T(4,128)}, u32[]{:S(2)}) copy-start(s32[128,4]{0,1:T(4,128)} %param.23) | copy-start | bytes 6148
  118.2 90.8 %copy-start.7 = (f32[128,4]{0,1:T(4,128)S(1)}, f32[128,4]{0,1:T(4,128)}, u32[]{:S(2)}) copy-start(f32[128,4]{0,1:T(4,128)} %param.24) | copy-start | bytes 6148
  203.1 124.6 %copy-start.8 = (f32[1024]{0:T(1024)S(1)}, f32[1024]{0:T(1024)}, u32[]{:S(2)}) copy-start(f32[1024]{0:T(1024)} %param.19) | copy-start | bytes 12292
  204.2 10.8 %all-to-all-start = ((bf16[8,64,128]{2,1,0:T(8,128)(2,1)}), bf16[8,64,128]{2,1,0:T(8,128)(2,1)S(1)}, u32[]{:S(2)}, u32[]{:S(2)}) async-start(bf16[8,64,128]{2,1,0:T(8,128)(2,1)} %copy.38), calls=%async_computation | async-start | bytes 262144 | tf_op jit(solution)/shard_map/all_to_all | solution.py:164
  214.9 129.0 %all-to-all-start.3 = ((bf16[256,32,32]{0,2,1:T(8,128)(2,1)}), bf16[256,32,32]{0,2,1:T(8,128)(2,1)S(1)}, u32[]{:S(2)}, u32[]{:S(2)}) async-start(bf16[256,32,32]{0,2,1:T(8,128)(2,1)} %bitcast.33), calls=%async_computation.3 | async-start | bytes 1048576 | tf_op jit(solution)/shard_map/all_to_all | solution.py:205
Sparse Core Ops, SparseCore 0:
  49.2 55.7 all-gather.3
